TPU v7x, 32 devices: a whole 2x2x4 slice. The times are simulated.
32 devices in a mesh: sp: 16 (over z, y, core), dp: 2 (over x).
Axes of the slice: x: 2, y: 2, z: 4, core: 2. Of those that a mesh axis runs over, the one named last changes fastest.
Arguments:
- signal: bfloat16 [2, 2048, 1024], P('dp', 'sp'), may hold values from -6 to 6
- pace: float32 [2, 16], P('dp'), may hold values from 0.5 to 2
- log_step: float32 [64], P('sp'), may hold values from -5.52 to -4.42
- a_real: float32 [64, 64], P('sp'), may hold values from -4 to -0.002, as said below
- a_imag: float32 [64, 64], P('sp'), may hold values from 0.5 to 201.06177
- in_map: float32 [64, 2, 64, 16], P('sp'), may hold values from -3 to 3
- out_map: float32 [64, 2, 16, 64], P('sp'), may hold values from -0.5 to 0.5
- skip: float32 [1024], P('sp'), may hold values from -1 to 1
- init_state: float32 [2, 2, 64, 64], P('dp', None, 'sp'), may hold values from -5 to 5
- w_glu: bfloat16 [1024, 1024], P('sp', 'dp'), may hold values from -0.1875 to 0.1875
- b_glu: float32 [1024], replicated, may hold values from -4 to 4
- g_mix: float32 [1024], replicated, may hold values from 0.1 to 1.9
- w_out: bfloat16 [1024, 4096], P('sp', 'dp'), may hold values from -0.1875 to 0.1875
Outputs:
- result: bfloat16 [2, 2048, 4096], P('dp', 'sp')
Inputs may be any that keep to these rules, and one draw needn't show every extreme that they name: `a_real`: negative entries; within a group all entries are of one order.
All inputs are finite; a program needn't handle non-finite values.
Results may differ from a plain program's by a relative error of at most 0.0075.
Values may be sent and summed in bfloat16 or wider, within the bound.
No kernel may reach another device: no remote copies, remote signals or barrier semaphores. Data moves between devices by JAX's collectives and lax.ppermute only.
A program may use at most 64 MiB of HBM per device.

v0:
```python
import jax
import jax.numpy as jnp
from jax import lax
from jax.sharding import PartitionSpec as P


def combine(first, second):
    a1r, a1i, b1r, b1i = first
    a2r, a2i, b2r, b2i = second
    return (
        a2r * a1r - a2i * a1i,
        a2r * a1i + a2i * a1r,
        a2r * b1r - a2i * b1i + b2r,
        a2r * b1i + a2i * b1r + b2i,
    )


def mix_group(series, pace_row, log_rate, a_re, a_im, in_map, out_map, skip_row, init):
    blocks_count = pace_row.shape[0]
    length = series.shape[0]
    span = length // blocks_count
    states = a_re.shape[0]
    steps = (jnp.exp(log_rate) * pace_row)[:, None]
    decay = jnp.exp(a_re * steps)
    bar_re = decay * jnp.cos(a_im * steps)
    bar_im = decay * jnp.sin(a_im * steps)
    modulus = a_re * a_re + a_im * a_im
    coef_re = ((bar_re - 1.0) * a_re + bar_im * a_im) / modulus
    coef_im = (bar_im * a_re - (bar_re - 1.0) * a_im) / modulus
    drive_re = coef_re[..., None] * in_map[0] - coef_im[..., None] * in_map[1]
    drive_im = coef_re[..., None] * in_map[1] + coef_im[..., None] * in_map[0]
    drive = jnp.concatenate([drive_re, drive_im], axis=1).astype(jnp.bfloat16)
    blocks = series.reshape(blocks_count, span, series.shape[1])
    inject = jnp.einsum("kpc,ksc->kps", drive, blocks, preferred_element_type=jnp.float32)
    inner_re = inject[:, :states]
    inner_im = inject[:, states:]
    power_re = bar_re[..., None]
    power_im = bar_im[..., None]
    offset = 1
    while offset < span:
        moved_re = jnp.pad(inner_re[..., :-offset], ((0, 0), (0, 0), (offset, 0)))
        moved_im = jnp.pad(inner_im[..., :-offset], ((0, 0), (0, 0), (offset, 0)))
        inner_re, inner_im = (
            inner_re + power_re * moved_re - power_im * moved_im,
            inner_im + power_re * moved_im + power_im * moved_re,
        )
        power_re, power_im = (power_re * power_re - power_im * power_im, 2.0 * power_re * power_im)
        offset = offset * 2
    ends_re = (
        inner_re[:, :, -1].at[0].add(power_re[0, :, 0] * init[0] - power_im[0, :, 0] * init[1])
    )
    ends_im = (
        inner_im[:, :, -1].at[0].add(power_re[0, :, 0] * init[1] + power_im[0, :, 0] * init[0])
    )
    carried = lax.associative_scan(
        combine, (power_re[..., 0], power_im[..., 0], ends_re, ends_im), axis=0
    )
    before_re = jnp.concatenate([init[0][None], carried[2][:-1]], axis=0)[..., None]
    before_im = jnp.concatenate([init[1][None], carried[3][:-1]], axis=0)[..., None]
    places = (jnp.arange(span, dtype=jnp.float32) + 1.0)[None, None, :]
    scaled = steps[:, :, None] * places
    magnitude = jnp.exp(a_re[None, :, None] * scaled)
    angle = a_im[None, :, None] * scaled
    lift_re = magnitude * jnp.cos(angle)
    lift_im = magnitude * jnp.sin(angle)
    state_re = inner_re + lift_re * before_re - lift_im * before_im
    state_im = inner_im + lift_re * before_im + lift_im * before_re
    highest = lax.Precision.HIGHEST
    response = jnp.einsum("cp,kps->ksc", out_map[0], state_re, precision=highest) - jnp.einsum(
        "cp,kps->ksc", out_map[1], state_im, precision=highest
    )
    response = response.reshape(length, series.shape[1]) + skip_row * series.astype(jnp.float32)
    return jax.nn.gelu(response).astype(jnp.bfloat16)


def folder(left, piece):
    return jnp.dot(left, piece, preferred_element_type=jnp.float32)


def per_device(
    signal,
    pace,
    log_step,
    a_real,
    a_imag,
    in_map,
    out_map,
    skip,
    init_state,
    w_glu,
    b_glu,
    g_mix,
    w_out,
):
    local_seqs = signal.shape[0]
    tokens = signal.shape[1]
    width = signal.shape[2]
    groups = a_real.shape[0]
    channels = width // (groups * lax.axis_size("sp"))
    grouped = lax.all_to_all(signal, "sp", split_axis=2, concat_axis=1, tiled=True)
    length = grouped.shape[1]
    skips = skip.reshape(groups, channels)

    def per_sequence(inputs):
        sample, pace_row, init_row = inputs
        series = sample.reshape(length, groups, channels)
        outputs = jax.vmap(mix_group, in_axes=(1, None, 0, 0, 0, 0, 0, 0, 1), out_axes=1)(
            series, pace_row, log_step, a_real, a_imag, in_map, out_map, skips, init_row
        )
        return outputs.reshape(length, groups * channels)

    local_act = lax.map(per_sequence, (grouped, pace, init_state))
    activated = lax.all_to_all(local_act, "sp", split_axis=1, concat_axis=2, tiled=True)
    rows = activated.reshape(local_seqs * tokens, width)
    glu_cols, out_cols = (
        lax.all_gather(w_glu, "dp", axis=1, tiled=True),
        lax.all_gather(w_out, "dp", axis=1, tiled=True),
    )
    gate_pre = folder(rows, lax.all_gather(glu_cols, "sp", axis=0, tiled=True)) + b_glu
    gated = rows.astype(jnp.float32) * jax.nn.sigmoid(gate_pre)
    scale = lax.rsqrt(jnp.mean(gated * gated, axis=-1, keepdims=True) + 1e-06)
    mixed = (gated * scale * g_mix).astype(jnp.bfloat16)
    output = folder(mixed, lax.all_gather(out_cols, "sp", axis=0, tiled=True)).astype(jnp.bfloat16)
    return output.reshape(local_seqs, tokens, output.shape[1])


def solution(mesh):
    in_specs = (
        P("dp", "sp", None),
        P("dp", None),
        P("sp"),
        P("sp", None),
        P("sp", None),
        P("sp", None, None, None),
        P("sp", None, None, None),
        P("sp"),
        P("dp", None, "sp", None),
        P("sp", "dp"),
        P(),
        P(),
        P("sp", "dp"),
    )
    out_specs = P("dp", "sp", None)
    return jax.shard_map(
        per_device, mesh=mesh, in_specs=in_specs, out_specs=out_specs, check_vma=False
    )
```

profile of v0, /device:TPU:0, one launch (start us, length us, event | category | flops | bytes accessed | tf_op | source)
XLA Modules:
  0.0 147.8 jit_solution(5512769175658030008)
XLA Ops:
  6.5 7.8 %all_gather.12 = bf16[64,1024]{1,0:T(8,128)(2,1)} all-gather(bf16[64,512]{1,0:T(8,128)(2,1)} %param.26), channel_id=1, replica_groups=mesh['sp'=16,'dp'=2] {'dp'}, dimensions={1}, use_global_device_ids=true | all-gather | bytes 196608 | tf_op jit(solution)/shard_map/all_gather | solution.py:116
  14.4 8.4 %all_gather.14 = bf16[64,4096]{1,0:T(8,128)(2,1)} all-gather(bf16[64,2048]{1,0:T(8,128)(2,1)} %param.29), channel_id=1, replica_groups=mesh['sp'=16,'dp'=2] {'dp'}, dimensions={1}, use_global_device_ids=true | all-gather | bytes 786432 | tf_op jit(solution)/shard_map/all_gather | solution.py:117
  22.8 1.3 copy.90
  24.1 0.5 broadcast.764
  24.6 2.2 %reduce.14 = bf16[1024,128]{1,0:T(8,128)(2,1)S(1)} reduce(bf16[1024,1,128]{2,1,0:T(2,128)(2,1)S(1)} %bitcast.149, bf16[]{:T(256)} %broadcast.764), dimensions={1}, to_apply=%bitcast.92.reduce_sub_computation | reduce | bytes 524290
  26.8 0.8 reshape.452
  27.5 6.2 %all-to-all-start = ((bf16[16,2,4096]{2,1,0:T(2,128)(2,1)}), bf16[16,2,4096]{2,1,0:T(2,128)(2,1)S(1)}, u32[]{:S(2)}, u32[]{:S(2)}) async-start(bf16[16,2,4096]{2,1,0:T(2,128)(2,1)} %reshape.452), calls=%async_computation | async-start | bytes 524288 | tf_op jit(solution)/shard_map/all_to_all | solution.py:100
  34.0 0.3 multiply_sine_fusion.2
  34.4 0.3 broadcast_multiply_fusion.4
  35.7 8.1 %all-to-all-done = bf16[16,2,4096]{2,1,0:T(2,128)(2,1)S(1)} async-done(((bf16[16,2,4096]{2,1,0:T(2,128)(2,1)}), bf16[16,2,4096]{2,1,0:T(2,128)(2,1)S(1)}, u32[]{:S(2)}, u32[]{:S(2)}) %all-to-all-start) | async-done | bytes 262176 | tf_op jit(solution)/shard_map/all_to_all | solution.py:100
  44.4 1.4 fusion.48
  45.9 0.6 fusion.80
  46.5 2.5 %fusion.4 = (f32[4,16,64,128]{3,2,1,0:T(8,128)S(1)}, f32[4,16,64,128]{3,2,1,0:T(8,128)S(1)}) fusion(f32[4,16,128,128]{3,2,1,0:T(8,128)S(1)} %fusion.48, f32[4,16,64,127]{3,2,1,0:T(8,128)S(1)} %get-tuple-element.102, f32[4,16,64,127]{3,2,1,0:T(8,128)S(1)} %get-tuple-element.101, f32[4,16,64]{2,1,0:T(8,128)S(1)} %get-tuple-element.151, ...), kind=kLoop, calls=%fused_computation.11 | loop fusion | flops 4194304 | bytes 12582912 | tf_op jit(solution)/shard_map/while/body/eval_jaxpr/vmap()/sub | solution.py:44
  49.0 2.5 %multiply_subtract_fusion.5 = (f32[4,16,64,128]{3,2,1,0:T(8,128)S(1)}, f32[4,16,64,128]{3,2,1,0:T(8,128)S(1)}) fusion(f32[4,16,64,128]{3,2,1,0:T(8,128)S(1)} %get-tuple-element.87, f32[4,16,64,126]{3,2,1,0:T(8,128)S(1)} %bitcast.135, f32[4,16,64,126]{3,2,1,0:T(8,128)S(1)} %bitcast.134, f32[4,16,64]{2,1,0:T(8,128)S(1)} %get-tuple-element.152, ...), kind=kLoop, calls=%fused_computation.34 | loop fusion | flops 4194304 | bytes 12550144 | tf_op jit(solution)/shard_map/while/body/eval_jaxpr/vmap()/sub | solution.py:44
  51.5 2.5 %multiply_subtract_fusion.4 = (f32[4,16,64,128]{3,2,1,0:T(8,128)S(1)}, f32[4,16,64,128]{3,2,1,0:T(8,128)S(1)}) fusion(f32[4,16,64,128]{3,2,1,0:T(8,128)S(1)} %get-tuple-element.99, f32[4,16,64,124]{3,2,1,0:T(8,128)S(1)} %bitcast.139, f32[4,16,64,124]{3,2,1,0:T(8,128)S(1)} %bitcast.138, f32[4,16,64]{2,1,0:T(8,128)S(1)} %get-tuple-element.148, ...), kind=kLoop, calls=%fused_computation.32 | loop fusion | flops 4194304 | bytes 12484608 | tf_op jit(solution)/shard_map/while/body/eval_jaxpr/vmap()/sub | solution.py:44
  54.1 2.5 %multiply_subtract_fusion.3 = (f32[4,16,64,128]{3,2,1,0:T(8,128)S(1)}, f32[4,16,64,128]{3,2,1,0:T(8,128)S(1)}) fusion(f32[4,16,64,128]{3,2,1,0:T(8,128)S(1)} %get-tuple-element.97, f32[4,16,64,120]{3,2,1,0:T(8,128)S(1)} %bitcast.141, f32[4,16,64,120]{3,2,1,0:T(8,128)S(1)} %bitcast.140, f32[4,16,64]{2,1,0:T(8,128)S(1)} %get-tuple-element.146, ...), kind=kLoop, calls=%fused_computation.30 | loop fusion | flops 4194304 | bytes 12353536 | tf_op jit(solution)/shard_map/while/body/eval_jaxpr/vmap()/sub | solution.py:44
  56.6 2.5 %multiply_subtract_fusion.2 = (f32[4,16,64,128]{3,2,1,0:T(8,128)S(1)}, f32[4,16,64,128]{3,2,1,0:T(8,128)S(1)}) fusion(f32[4,16,64,128]{3,2,1,0:T(8,128)S(1)} %get-tuple-element.95, f32[4,16,64,112]{3,2,1,0:T(8,128)S(1)} %bitcast.143, f32[4,16,64,112]{3,2,1,0:T(8,128)S(1)} %bitcast.142, f32[4,16,64]{2,1,0:T(8,128)S(1)} %get-tuple-element.144, ...), kind=kLoop, calls=%fused_computation.28 | loop fusion | flops 4194304 | bytes 12091392 | tf_op jit(solution)/shard_map/while/body/eval_jaxpr/vmap()/sub | solution.py:44
  59.1 2.5 %multiply_subtract_fusion.1 = (f32[4,16,64,128]{3,2,1,0:T(8,128)S(1)}, f32[4,16,64,128]{3,2,1,0:T(8,128)S(1)}) fusion(f32[4,16,64,128]{3,2,1,0:T(8,128)S(1)} %get-tuple-element.93, f32[4,16,64,96]{3,2,1,0:T(8,128)S(1)} %bitcast.145, f32[4,16,64,96]{3,2,1,0:T(8,128)S(1)} %bitcast.144, f32[4,16,64]{2,1,0:T(8,128)S(1)} %get-tuple-element.142, ...), kind=kLoop, calls=%fused_computation.26 | loop fusion | flops 4194304 | bytes 11567104 | tf_op jit(solution)/shard_map/while/body/eval_jaxpr/vmap()/sub | solution.py:44
  61.7 2.5 %multiply_subtract_fusion = (f32[4,16,64,128]{3,2,1,0:T(8,128)S(1)}, f32[4,16,64,128]{3,2,1,0:T(8,128)S(1)}) fusion(f32[4,16,64,128]{3,2,1,0:T(8,128)S(1)} %get-tuple-element.91, f32[4,16,64,64]{3,2,1,0:T(8,128)S(1)} %bitcast.137, f32[4,16,64,64]{3,2,1,0:T(8,128)S(1)} %bitcast.136, f32[4,16,64]{2,1,0:T(8,128)S(1)} %get-tuple-element.140, ...), kind=kLoop, calls=%fused_computation.24 | loop fusion | flops 4194304 | bytes 10518528 | tf_op jit(solution)/shard_map/while/body/eval_jaxpr/vmap()/sub | solution.py:44
  64.5 2.2 %slice_reduce_fusion = (f32[4,16,64]{2,1,0:T(8,128)S(1)}, f32[4,16,64]{2,1,0:T(8,128)S(1)}) fusion(f32[4,16,64,128]{3,2,1,0:T(8,128)S(1)} %get-tuple-element.90, f32[4,16,64,128]{3,2,1,0:T(8,128)S(1)} %get-tuple-element.89), kind=kLoop, calls=%fused_computation.6 | loop fusion | bytes 65536 | tf_op jit(solution)/shard_map/while/body/eval_jaxpr/vmap()/slice | solution.py:53
  68.6 11.0 %fusion.5 = f32[4,16,128,16]{2,3,1,0:T(8,128)S(1)} fusion(f32[4,16,64,128]{3,2,1,0:T(8,128)} %copy-done, f32[4,16,64]{2,1,0:T(8,128)S(1)} %pad_maximum_fusion.1, f32[4,16,64]{2,1,0:T(8,128)S(1)} %pad_maximum_fusion, f32[4,64]{1,0:T(4,128)S(1)} %copy-done.3, f32[4,16,128]{2,1,0:T(8,128)S(1)} %broadcast_multiply_fusion.6, f32[4,64]{1,0:T(4,128)S(1)} %copy-done.4, ...), kind=kOutput, calls=%fused_computation.12 | convolution fusion | flops 104857600 | bytes 2756608 | tf_op jit(solution)/shard_map/while/body/eval_jaxpr/vmap(cp,kps->ksc)/dot_general | solution.py:69
  79.6 9.9 %fusion.22 = f32[4,16,2,8,128]{4,3,2,1,0:T(8,128)S(1)} fusion(f32[4,16,128,16]{2,3,1,0:T(8,128)S(1)} %fusion.5, f32[4,16,64,128]{3,2,1,0:T(8,128)S(1)} %get-tuple-element.89, f32[4,16,64]{2,1,0:T(8,128)S(1)} %pad_maximum_fusion.1, f32[4,16,64]{2,1,0:T(8,128)S(1)} %pad_maximum_fusion, f32[4,64]{1,0:T(4,128)S(1)} %copy-done.3, ...), kind=kOutput, calls=%fused_computation.36 | convolution fusion | flops 104988672 | bytes 3280896 | tf_op jit(solution)/shard_map/while/body/eval_jaxpr/vmap(cp,kps->ksc)/dot_general | solution.py:69
  89.6 0.3 fusion.47
  89.9 0.7 copy.127
  90.6 11.4 %reduce.15 = bf16[2048,64]{1,0:T(8,128)(2,1)S(1)} reduce(bf16[2048,1,64]{2,1,0:T(2,128)(2,1)S(1)} %bitcast.147, bf16[]{:T(256)} %broadcast.764), dimensions={1}, to_apply=%bitcast.94.reduce_sub_computation | reduce | bytes 524290
  102.1 0.4 reshape.454
  102.5 20.1 %all_to_all.30 = bf16[16,2,4096]{2,1,0:T(2,128)(2,1)S(1)} all-to-all(bf16[16,2,4096]{2,1,0:T(2,128)(2,1)S(1)} %reshape.454), channel_id=1, replica_groups=mesh['sp'=16,'dp'=2] {'sp'}, dimensions={0} | all-to-all | bytes 524288 | tf_op jit(solution)/shard_map/all_to_all | solution.py:113
  122.6 0.6 reshape.455
  123.2 0.6 copy.128
  124.2 2.2 %multiply_reduce_fusion = (f32[128]{0:T(128)S(1)}, f32[128,1024]{1,0:T(8,128)S(1)}) fusion(f32[1024]{0:T(1024)S(1)} %copy-done.9, bf16[128,1024]{0,1:T(8,128)(2,1)S(1)} %bitcast.153, bf16[1024,1024]{1,0:T(8,128)(2,1)} %all-gather.3.cloned.1.call-done, bf16[128,1024]{1,0:T(8,128)(2,1)S(1)} %copy.130), kind=kOutput, calls=%fused_computation.64 | convolution fusion | flops 269483904 | bytes 3150336 | tf_op jit(solution)/shard_map/dot_general | solution.py:77
  126.4 8.8 %all-gather.5.cloned.1.call-done = bf16[1024,4096]{1,0:T(8,128)(2,1)} async-done(((bf16[64,4096]{1,0:T(8,128)(2,1)}), bf16[1024,4096]{1,0:T(8,128)(2,1)}) %all-gather.5.cloned.1.call-update) | async-done | bytes 8388624 | tf_op jit(solution)/shard_map/all_gather | solution.py:123
  135.3 5.7 %fusion = bf16[1,128,4096]{2,1,0:T(8,128)(2,1)} fusion(bf16[1024,4096]{1,0:T(8,128)(2,1)} %all-gather.5.cloned.1.call-done, f32[128,1024]{1,0:T(8,128)S(1)} %get-tuple-element.161, f32[1024]{0:T(1024)S(1)} %copy-done.1, f32[128]{0:T(128)S(1)} %add_rsqrt_fusion), kind=kOutput, calls=%fused_computation.1 | convolution fusion | flops 1074659328 | bytes 9966080 | tf_op jit(solution)/shard_map/dot_general | solution.py:77
  (132 shorter events, 4.1 us)
Async XLA Ops:
  6.5 27.2 %copy-start.10 = (f32[4]{0:T(128)S(1)}, f32[4]{0:T(128)}, u32[]{:S(2)}) copy-start(f32[4]{0:T(128)} %param.19) | copy-start | bytes 52
  6.5 27.2 %copy-start.7 = (f32[1,16]{1,0:T(1,128)S(1)}, f32[1,16]{1,0:T(1,128)}, u32[]{:S(2)}) copy-start(f32[1,16]{1,0:T(1,128)} %param.18) | copy-start | bytes 196
  6.5 27.4 %copy-start.4 = (f32[4,64]{1,0:T(4,128)S(1)}, f32[4,64]{1,0:T(4,128)}, u32[]{:S(2)}) copy-start(f32[4,64]{1,0:T(4,128)} %param.20) | copy-start | bytes 3076
  6.5 117.6 %all-gather.3.cloned.1.call-start = ((), (), s32[]{:S(2)}) async-start(), calls=%async_computation.2 | async-start | bytes 2228224 | tf_op jit(solution)/shard_map/all_gather | solution.py:119
  14.3 19.7 %copy-start.3 = (f32[4,64]{1,0:T(4,128)S(1)}, f32[4,64]{1,0:T(4,128)}, u32[]{:S(2)}) copy-start(f32[4,64]{1,0:T(4,128)} %param.21) | copy-start | bytes 3076
  14.3 120.9 %all-gather.5.cloned.1.call-start = ((), (), s32[]{:S(2)}) async-start(), calls=%async_computation.3 | async-start | bytes 8912896 | tf_op jit(solution)/shard_map/all_gather | solution.py:123
  24.1 11.3 %copy-start.5 = (f32[1,2,4,64]{3,2,1,0:T(4,128)S(1)}, f32[1,2,4,64]{3,2,1,0:T(4,128)}, u32[]{:S(2)}) copy-start(f32[1,2,4,64]{3,2,1,0:T(4,128)} %param.25) | copy-start | bytes 6148
  24.6 10.9 %copy-start.6 = (f32[64]{0:T(128)S(1)}, f32[64]{0:T(128)}, u32[]{:S(2)}) copy-start(f32[64]{0:T(128)} %param.24) | copy-start | bytes 772
  24.6 11.0 %copy-start.2 = (f32[4,2,64,16]{2,3,1,0:T(8,128)S(1)}, f32[4,2,64,16]{2,3,1,0:T(8,128)}, u32[]{:S(2)}) copy-start(f32[4,2,64,16]{2,3,1,0:T(8,128)} %param.22) | copy-start | bytes 98308
  27.5 16.3 %all-to-all-start = ((bf16[16,2,4096]{2,1,0:T(2,128)(2,1)}), bf16[16,2,4096]{2,1,0:T(2,128)(2,1)S(1)}, u32[]{:S(2)}, u32[]{:S(2)}) async-start(bf16[16,2,4096]{2,1,0:T(2,128)(2,1)} %reshape.452), calls=%async_computation | async-start | bytes 524288 | tf_op jit(solution)/shard_map/all_to_all | solution.py:100
  64.2 2.6 %copy-start = (f32[4,16,64,128]{3,2,1,0:T(8,128)}, f32[4,16,64,128]{3,2,1,0:T(8,128)S(1)}, u32[]{:S(2)}) copy-start(f32[4,16,64,128]{3,2,1,0:T(8,128)S(1)} %get-tuple-element.90) | copy-start | bytes 6291460
  66.7 1.8 %copy-start.8 = (f32[4,2,16,64]{3,2,1,0:T(8,128)S(1)}, f32[4,2,16,64]{3,2,1,0:T(8,128)}, u32[]{:S(2)}) copy-start(f32[4,2,16,64]{3,2,1,0:T(8,128)} %param.23) | copy-start | bytes 98308
  122.6 1.6 %copy-start.9 = (f32[1024]{0:T(1024)S(1)}, f32[1024]{0:T(1024)}, u32[]{:S(2)}) copy-start(f32[1024]{0:T(1024)} %param.27) | copy-start | bytes 12292
  124.1 11.2 %copy-start.1 = (f32[1024]{0:T(1024)S(1)}, f32[1024]{0:T(1024)}, u32[]{:S(2)}) copy-start(f32[1024]{0:T(1024)} %param.28) | copy-start | bytes 12292
Sparse Core Ops, SparseCore 0:
  14.5 41.9 all-gather.2
  58.6 76.6 all-gather.4
where the time goes:
time: 148 us
  blocking collectives  36.3 us (25%)
  other arithmetic  33.4 us (23%)
  matrix products  30.3 us (20%)
  waiting for transfers between devices  17 us (11%)
  between operations  14.1 us (10%)
  local copies, waits for them, and re-layouts  10.5 us (7%)
  starting transfers between devices  6.23 us (4%)
    all_to_all x1, blocking collectives, per_device(): lax.all_to_all(local_act, 'sp', split_axis=1, concat_axis=2, tiled=True)  20.1 us
    sub x7, other arithmetic, mix_group(): inner_re + power_re * moved_re - power_im * moved_im  17.7 us
    unnamed x2, other arithmetic  13.6 us
    dot_general x1, matrix products, mix_group(): jnp.einsum('cp,kps->ksc', out_map[1], state_im, precision=highest)  11 us
    dot_general x1, matrix products, mix_group(): jnp.einsum('cp,kps->ksc', out_map[0], state_re, precision=highest)  9.95 us
    all_gather x1, waiting for transfers between devices, per_device(): lax.all_gather(out_cols, 'sp', axis=0, tiled=True)  8.84 us
    all_gather x1, blocking collectives, per_device(): lax.all_gather(w_out, 'dp', axis=1, tiled=True)  8.38 us
    all_to_all x1, waiting for transfers between devices, per_device(): lax.all_to_all(signal, 'sp', split_axis=2, concat_axis=1, tiled=True)  8.07 us
  transfers between devices with their start and end apart: 3, of which 2 were waited for; matrix products, arithmetic and copies ran while one was open for 46% of the time, Pallas kernels for 0%

commit v1 on v0

v1 whole, which is shorter than its diff:
```python
import functools

import jax
import jax.numpy as jnp
from jax import lax
from jax.experimental import pallas as pl
from jax.experimental.pallas import tpu as pltpu
from jax.sharding import PartitionSpec as P

LANES = 128
OCT = 8
SMALL = 16
AXES = ("sp", "dp")
F32 = jnp.float32
BF16 = jnp.bfloat16
VMEM = pltpu.VMEM
LIMIT = 60 * 1024 * 1024


class Plan:
    def __init__(self, mesh, signal, pace, a_real, w_glu, w_out):
        self.sp = mesh.shape["sp"]
        self.X = mesh.shape["dp"]
        self.C = 2 if self.sp % 2 == 0 else 1
        self.Y = 2 if self.sp % (2 * self.C) == 0 else 1
        self.Q = self.C * self.Y
        self.Z = self.sp // self.Q
        self.T = signal.shape[1]
        self.width = signal.shape[2]
        self.gl = a_real.shape[0]
        self.states = a_real.shape[1]
        self.chl = self.width // self.sp
        self.ch = self.chl // self.gl
        self.ng = self.gl * self.Z
        self.noct = self.ng // OCT
        self.rows = self.Q * self.noct
        self.mine = self.Z * self.chl
        self.maprows = self.gl * self.ch
        self.packed = 2 * self.maprows + 3 * SMALL
        self.wr = w_out.shape[0]
        self.wc = w_out.shape[1] // self.C
        self.gc = w_glu.shape[1]
        if signal.shape[0] != 1 or pace.shape[1] != self.sp or self.ng % OCT:
            raise ValueError("unsupported sizes")
        if self.states * 2 != LANES or self.ch * OCT != LANES or 3 * self.gl >= SMALL:
            raise ValueError("unsupported sizes")

    def place(self):
        s = lax.axis_index("sp")
        x = lax.axis_index("dp")
        q = lax.rem(s, self.Q)
        z = lax.div(s, self.Q)
        c = lax.rem(q, self.C)
        y = lax.div(q, self.C)
        return z, y, c, x, q

    def pairs(self, move):
        out = []
        for s in range(self.sp):
            for x in range(self.X):
                q, z = s % self.Q, s // self.Q
                c, y = q % self.C, q // self.C
                z2, y2, c2, x2 = move(z, y, c, x)
                t = (z2 * self.Y + y2) * self.C + c2
                out.append((s * self.X + x, t * self.X + x2))
        return out

    def shift_z(self, k):
        return self.pairs(lambda z, y, c, x: ((z + k) % self.Z, y, c, x))

    def swap_q(self, j):
        def move(z, y, c, x):
            q = (y * self.C + c) ^ j
            return z, q // self.C, q % self.C, x

        return self.pairs(move)

    def mixed(self, flip):
        def move(z, y, c, x):
            return (z, y ^ 1, c, x) if c ^ flip == 0 else (z, y, c, x ^ 1)

        return self.pairs(move)

    def shift_x(self, k):
        return self.pairs(lambda z, y, c, x: (z, y, c, (x + k) % self.X))

    def roles(self, y, c, x):
        if self.Y == 2 and self.X == 2:
            a = (1 - c) if self.C == 2 else 1
            b = 1 - a
            steps = [(0, 0), (a, b), (b, a), (1, 1)]
            return [(jnp.bitwise_xor(y, dy), jnp.bitwise_xor(x, dx)) for dy, dx in steps]
        out = []
        for m in range(self.X):
            for b in range(self.Y):
                out.append((jnp.bitwise_xor(y, b), lax.rem(x + (self.X - m), self.X)))
        return out

    def quad(self, unit):
        if self.Y == 2 and self.X == 2:
            other = send(unit, self.mixed(0))
            both = jnp.stack([unit, other])
            return [both, send(both, self.mixed(1))]
        both = jnp.stack([unit] + [send(unit, self.swap_q(self.C)) for _ in range(self.Y - 1)])
        return [both] + [send(both, self.shift_x(m)) for m in range(1, self.X)]


def send(value, pairs):
    return lax.ppermute(value, AXES, pairs)


def call(kernel, outs, scratch=(), flops=1_000_000, specs=None, **kw):
    return pl.pallas_call(
        kernel,
        out_shape=outs,
        scratch_shapes=list(scratch),
        **({} if specs is None else {"in_specs": specs}),
        compiler_params=pltpu.CompilerParams(vmem_limit_bytes=LIMIT),
        cost_estimate=pl.CostEstimate(flops=flops, bytes_accessed=1_000_000, transcendentals=0),
        **kw,
    )


def shape(dims, kind):
    return jax.ShapeDtypeStruct(dims, kind)


def pack_kernel(p, sig, in_map, out_map, a_re, a_im, log_step, init, skip, w_out, *rest):
    packed, keep, give = rest[0], rest[1], rest[2]
    pieces = rest[3 : 3 + p.Q]
    held, small = rest[3 + p.Q :]
    _, _, c, _, q = p.place()
    x = sig[0]
    for r in range(p.Q):
        slabs = [x[:, (z * p.Q + r) * p.chl : (z * p.Q + r + 1) * p.chl] for z in range(p.Z)]
        held[r] = jnp.concatenate(slabs, axis=1)
    for j in range(p.Q):
        pieces[j][...] = held[jnp.bitwise_xor(q, j)]
    n = p.maprows
    for g in range(p.gl):
        rows = slice(g * p.ch, (g + 1) * p.ch)
        both = jnp.concatenate([in_map[g, 0].T, in_map[g, 1].T], axis=1)
        packed[rows] = both.astype(BF16)
        both = jnp.concatenate([out_map[g, 0], out_map[g, 1]], axis=1)
        packed[n + g * p.ch : n + (g + 1) * p.ch] = both.astype(BF16)
    small[...] = jnp.zeros_like(small)
    small[0 : p.gl] = jnp.concatenate([a_re[...], a_im[...]], axis=1)
    small[p.gl : 2 * p.gl] = jnp.concatenate([init[0, 0], init[0, 1]], axis=1)
    small[2 * p.gl : 3 * p.gl] = jnp.broadcast_to(log_step[...], (p.gl, LANES))
    small[3 * p.gl : 3 * p.gl + 1, 0 : p.chl] = skip[...]
    value = small[...]
    high = value.astype(BF16)
    left = value - high.astype(F32)
    mid = left.astype(BF16)
    low = (left - mid.astype(F32)).astype(BF16)
    packed[2 * n : 2 * n + SMALL] = high
    packed[2 * n + SMALL : 2 * n + 2 * SMALL] = mid
    packed[2 * n + 2 * SMALL : 2 * n + 3 * SMALL] = low
    keep[...] = w_out[:, pl.ds(pl.multiple_of(c * p.wc, LANES), p.wc)]
    give[...] = w_out[:, pl.ds(pl.multiple_of((p.C - 1 - c) * p.wc, LANES), p.wc)]


def unpack(p, z, parts, prm):
    for k in range(p.Z):
        prm[lax.rem(z + (p.Z - k), p.Z)] = parts[k][...]
    n = 2 * p.maprows
    small = []
    for k in range(p.Z):
        high = prm[k, n : n + SMALL].astype(F32)
        mid = prm[k, n + SMALL : n + 2 * SMALL].astype(F32)
        low = prm[k, n + 2 * SMALL : n + 3 * SMALL].astype(F32)
        small.append(high + mid + low)
    return small


def spread(p, small, base, kind):
    lane = lax.broadcasted_iota(jnp.int32, (1, LANES), 1) < p.states
    out = []
    for o in range(p.noct):
        tiles = []
        for j in range(OCT // 2):
            first, second = (
                small[g // p.gl][base + g % p.gl : base + g % p.gl + 1]
                for g in (o * OCT + 2 * j, o * OCT + 2 * j + 1)
            )
            if kind == 0:
                second = pltpu.roll(second, p.states, 1)
            elif kind == 1:
                first = pltpu.roll(first, p.states, 1)
            tiles.append(jnp.where(lane, first, second))
        out.append(jnp.concatenate(tiles, axis=1))
    return jnp.concatenate(out, axis=0)


def block_matrix(p, prm, start, sign, o, out):
    per = OCT // p.gl
    parts = [prm[k, start : start + p.maprows] for k in range(o * per, (o + 1) * per)]
    x = jnp.concatenate(parts, axis=0).astype(F32)
    dims = (LANES, LANES)
    low = lax.broadcasted_iota(jnp.int32, dims, 1) < p.states
    lane_group = lax.broadcasted_iota(jnp.int32, dims, 1) // p.states
    row_group = lax.broadcasted_iota(jnp.int32, dims, 0) // p.ch
    turned = pltpu.roll(x, p.states, 1)
    real = jnp.where(low, x, turned)
    imag = jnp.where(low, turned, x) * sign
    half = OCT * p.states
    for j in range(OCT // 2):
        hit = row_group == lane_group + 2 * j
        at = j * LANES
        out[o, :, at : at + LANES] = jnp.where(hit, real, 0.0).astype(BF16)
        out[o, :, half + at : half + at + LANES] = jnp.where(hit, imag, 0.0).astype(BF16)


def power(a_re, a_im, span):
    size = jnp.exp(a_re * span)
    return size * jnp.cos(a_im * span), size * jnp.sin(a_im * span)


def times(ar, ai, br, bi):
    return ar * br - ai * bi, ar * bi + ai * br


def scan_kernel(p, pace, *refs):
    parts = refs[: p.Z]
    sigs = refs[p.Z : p.Z + p.Q]
    refs = refs[p.Z + p.Q :]
    outs, refs = refs[: p.Q], refs[p.Q :]
    ends, whole, bars, blocks, prods, starts, omat = refs[:7]
    prm, bmat, scr, order, porder = refs[7:]
    z, _, _, _, q = p.place()
    half = OCT * p.states
    small = unpack(p, z, parts, prm)
    are = spread(p, small, 0, 0)
    aim = spread(p, small, 0, 1)
    rate = jnp.exp(spread(p, small, 2 * p.gl, 2))
    starts[:, :half] = spread(p, small, p.gl, 0)
    starts[:, half:] = spread(p, small, p.gl, 1)
    steps = jnp.concatenate(
        [rate * pace[0, p.Q * z + jnp.bitwise_xor(q, j)] for j in range(p.Q)], axis=0
    )
    ar = jnp.concatenate([are] * p.Q, axis=0)
    ai = jnp.concatenate([aim] * p.Q, axis=0)
    br, bi = power(ar, ai, steps)
    bars[:, :half] = br
    bars[:, half:] = bi
    modulus = ar * ar + ai * ai
    cr = ((br - 1.0) * ar + bi * ai) / modulus
    ci = (bi * ar - (br - 1.0) * ai) / modulus
    pr, pi = power(ar, ai, steps * float(p.T))
    blocks[:, :half] = pr
    blocks[:, half:] = pi
    sums = []
    for k in range(p.Z):
        total = pace[0, p.Q * k]
        for j in range(1, p.Q):
            total = total + pace[0, p.Q * k + j]
        sums.append(rate * (total * float(p.T)))
    for k in range(p.Z):
        wr, wi = power(are, aim, sums[k])
        prods[k, :, :half] = wr
        prods[k, :, half:] = wi
    for o in range(p.noct):
        block_matrix(p, prm, 0, 1.0, o, bmat)
        block_matrix(p, prm, p.maprows, -1.0, o, omat)
    for j in range(p.Q):
        for o in range(p.noct):
            x = sigs[j][:, o * LANES : (o + 1) * LANES]
            got = jnp.dot(x, bmat[o], preferred_element_type=F32)
            r = j * p.noct + o
            for t in range(2 * half // LANES):
                scr[t, pl.ds(r, p.T, stride=p.rows), :] = got[:, t * LANES : (t + 1) * LANES]
    tiles = half // LANES

    def step(t, carry):
        at = pl.ds(pl.multiple_of(t * p.rows, p.rows), p.rows)
        new_re, new_im = [], []
        for m in range(tiles):
            s = slice(m * LANES, (m + 1) * LANES)
            xr = scr[m, at, :]
            xi = scr[tiles + m, at, :]
            sr, si = carry[m], carry[tiles + m]
            ur = cr[:, s] * xr - ci[:, s] * xi
            ui = cr[:, s] * xi + ci[:, s] * xr
            nr = (ur + br[:, s] * sr) - bi[:, s] * si
            ni = (ui + br[:, s] * si) + bi[:, s] * sr
            scr[m, at, :] = nr
            scr[tiles + m, at, :] = ni
            new_re.append(nr)
            new_im.append(ni)
        return tuple(new_re + new_im)

    zero = jnp.zeros((p.rows, LANES), F32)
    last = lax.fori_loop(0, p.T, step, (zero,) * (2 * tiles), unroll=4)
    final = jnp.concatenate(last, axis=1)
    ends[...] = final
    for j in range(p.Q):
        order[j] = final[j * p.noct : (j + 1) * p.noct]
        porder[j, :, :half] = pr[j * p.noct : (j + 1) * p.noct]
        porder[j, :, half:] = pi[j * p.noct : (j + 1) * p.noct]
    got = order[q]
    er, ei = got[:, :half], got[:, half:]
    for b in range(1, p.Q):
        at = jnp.bitwise_xor(q, b)
        got, by = order[at], porder[at]
        er, ei = times(by[:, :half], by[:, half:], er, ei)
        er, ei = er + got[:, :half], ei + got[:, half:]
    whole[:, :half] = er
    whole[:, half:] = ei
    skips = jnp.concatenate([small[k][3 * p.gl : 3 * p.gl + 1, : p.chl] for k in range(p.Z)], axis=1)
    for j in range(p.Q):
        for o in range(p.noct):
            y = answer(p, scr, omat, j, o)
            s = slice(o * LANES, (o + 1) * LANES)
            outs[j][:, s] = y + skips[:, s] * sigs[j][:, s].astype(F32)


def answer(p, scr, omat, j, o):
    r = j * p.noct + o
    n = 2 * OCT * p.states // LANES
    states = jnp.concatenate(
        [scr[t, pl.ds(r, p.T, stride=p.rows), :].astype(BF16) for t in range(n)], axis=1
    )
    return lax.dot_general(
        states, omat[o], (((1,), (1,)), ((), ())), preferred_element_type=F32
    )


def lift_kernel(p, ends, bars, blocks, prods, starts, omat, *refs):
    wholes = refs[: p.Z]
    bases = refs[p.Z : p.Z + p.Q]
    outs = refs[p.Z + p.Q : p.Z + 2 * p.Q]
    scr, seen, order = refs[p.Z + 2 * p.Q :]
    z, _, _, _, q = p.place()
    half = OCT * p.states
    for k in range(p.Z):
        seen[lax.rem(z + (p.Z - k), p.Z)] = wholes[k][...]
    vr, vi = starts[:, :half], starts[:, half:]
    for k in range(p.Z - 1):
        nr, ni = times(prods[k, :, :half], prods[k, :, half:], vr, vi)
        nr, ni = nr + seen[k, :, :half], ni + seen[k, :, half:]
        vr = jnp.where(k < z, nr, vr)
        vi = jnp.where(k < z, ni, vi)
    for j in range(p.Q):
        rows = slice(j * p.noct, (j + 1) * p.noct)
        order[0, j] = ends[rows, :]
        order[1, j] = blocks[rows, :]
    for b in range(p.Q):
        at = jnp.bitwise_xor(q, b)
        order[2, at, :, :half] = vr
        order[2, at, :, half:] = vi
        got, by = order[0, at], order[1, at]
        vr, vi = times(by[:, :half], by[:, half:], vr, vi)
        vr, vi = vr + got[:, :half], vi + got[:, half:]
    begin = jnp.concatenate([order[2, j] for j in range(p.Q)], axis=0)
    tiles = half // LANES
    bar = bars[...]

    def step(t, carry):
        at = pl.ds(pl.multiple_of(t * p.rows, p.rows), p.rows)
        new_re, new_im = [], []
        for m in range(tiles):
            br = bar[:, m * LANES : (m + 1) * LANES]
            bi = bar[:, half + m * LANES : half + (m + 1) * LANES]
            nr, ni = times(br, bi, carry[m], carry[tiles + m])
            scr[m, at, :] = nr
            scr[tiles + m, at, :] = ni
            new_re.append(nr)
            new_im.append(ni)
        return tuple(new_re + new_im)

    first = tuple(begin[:, t * LANES : (t + 1) * LANES] for t in range(2 * tiles))
    lax.fori_loop(0, p.T, step, first, unroll=4)
    for j in range(p.Q):
        for o in range(p.noct):
            s = slice(o * LANES, (o + 1) * LANES)
            v = answer(p, scr, omat, j, o) + bases[j][:, s]
            inner = 0.7978845608028654 * (v + 0.044715 * (v * v * v))
            outs[j][:, s] = (0.5 * v * (1.0 + jnp.tanh(inner))).astype(BF16)


def gate_kernel(p, count, b_glu, g_mix, *refs):
    pieces = refs[: p.Q]
    units = refs[p.Q : p.Q + count]
    out = refs[p.Q + count]
    held, weight = refs[p.Q + count + 1 :]
    z, y, c, x, q = p.place()
    for j in range(p.Q):
        held[jnp.bitwise_xor(q, j)] = pieces[j][...]
    slabs = [
        held[r][:, k * p.chl : (k + 1) * p.chl] for k in range(p.Z) for r in range(p.Q)
    ]
    act = jnp.concatenate(slabs, axis=1)
    per = count // p.C
    for side in range(p.C):
        owner = c if side == 0 else 1 - c
        roles = p.roles(y, owner, x)
        at = 0
        for n in range(per):
            unit = units[side * per + n]
            for i in range(unit.shape[0]):
                ys, xs = roles[at + i]
                for k in range(p.Z):
                    zs = lax.rem(z + (p.Z - k), p.Z)
                    row = ((zs * p.Y + ys) * p.C + owner) * p.wr
                    weight[
                        pl.ds(pl.multiple_of(row, p.wr), p.wr),
                        pl.ds(pl.multiple_of(xs * p.gc, LANES), p.gc),
                    ] = unit[i, k]
            at += unit.shape[0]
    pre = jnp.dot(act, weight[...], preferred_element_type=F32) + b_glu[...]
    gated = act.astype(F32) * jax.nn.sigmoid(pre)
    scale = lax.rsqrt(jnp.mean(gated * gated, axis=-1, keepdims=True) + 1e-06)
    out[...] = (gated * scale * g_mix[...]).astype(BF16)


def project_kernel(p, count, mixed, *refs):
    units = refs[:count]
    out = refs[count]
    (weight,) = refs[count + 1 :]
    z, y, c, x, _ = p.place()
    roles = p.roles(y, c, x)
    per = count // p.Z
    for k in range(p.Z):
        zs = lax.rem(z + (p.Z - k), p.Z)
        at = 0
        for n in range(per):
            unit = units[k * per + n]
            for i in range(unit.shape[0]):
                ys, xs = roles[at + i]
                for h in range(p.C):
                    owner = c if h == 0 else 1 - c
                    row = ((zs * p.Y + ys) * p.C + owner) * p.wr
                    weight[xs, pl.ds(pl.multiple_of(row, p.wr), p.wr), :] = unit[
                        i, h * p.wr : (h + 1) * p.wr
                    ]
            at += unit.shape[0]
    rows = mixed[...]
    for n in range(p.X):
        got = jnp.dot(rows, weight[n], preferred_element_type=F32)
        out[:, n * p.wc : (n + 1) * p.wc] = got.astype(BF16)


def merge_kernel(p, *refs):
    halves, out = refs[: p.C], refs[p.C]
    _, _, c, _, _ = p.place()
    for h in range(p.C):
        owner = c if h == 0 else 1 - c
        for n in range(p.X):
            at = pl.multiple_of((n * p.C + owner) * p.wc, LANES)
            out[0, :, pl.ds(at, p.wc)] = halves[h][:, n * p.wc : (n + 1) * p.wc]


def layer(
    mesh,
    signal,
    pace,
    log_step,
    a_real,
    a_imag,
    in_map,
    out_map,
    skip,
    init_state,
    w_glu,
    b_glu,
    g_mix,
    w_out,
):
    p = Plan(mesh, signal, pace, a_real, w_glu, w_out)
    half = OCT * p.states
    packed, keep, give, *pieces = call(
        functools.partial(pack_kernel, p),
        [shape((p.packed, LANES), BF16), shape((p.wr, p.wc), BF16), shape((p.wr, p.wc), BF16)]
        + [shape((p.T, p.mine), BF16)] * p.Q,
        [VMEM((p.Q, p.T, p.mine), BF16), VMEM((SMALL, LANES), F32)],
    )(
        signal,
        in_map,
        out_map,
        a_real,
        a_imag,
        log_step.reshape(p.gl, 1),
        init_state,
        skip.reshape(1, p.chl),
        w_out,
    )
    unit = keep
    if p.C == 2:
        unit = jnp.concatenate([keep, send(give, p.swap_q(1))], axis=0)
    parts = [packed] + [send(packed, p.shift_z(k)) for k in range(1, p.Z)]
    sigs = [pieces[0]] + [send(pieces[j], p.swap_q(j)) for j in range(1, p.Q)]
    glu = jnp.stack([w_glu] + [send(w_glu, p.shift_z(k)) for k in range(1, p.Z)])
    glu_units = p.quad(glu)
    if p.C == 2:
        glu_units = glu_units + [send(u, p.swap_q(1)) for u in glu_units]
    out_units = []
    for k in range(p.Z):
        out_units += p.quad(unit)
        if k + 1 < p.Z:
            unit = send(unit, p.shift_z(1))

    smem = pl.BlockSpec(memory_space=pltpu.SMEM)
    vmem = pl.BlockSpec(memory_space=VMEM)
    results = call(
        functools.partial(scan_kernel, p),
        [shape((p.T, p.mine), F32)] * p.Q
        + [
            shape((p.rows, 2 * half), F32),
            shape((p.noct, 2 * half), F32),
            shape((p.rows, 2 * half), F32),
            shape((p.rows, 2 * half), F32),
            shape((p.Z, p.noct, 2 * half), F32),
            shape((p.noct, 2 * half), F32),
            shape((p.noct, LANES, 2 * half), BF16),
        ],
        [
            VMEM((p.Z, p.packed, LANES), BF16),
            VMEM((p.noct, LANES, 2 * half), BF16),
            VMEM((2 * half // LANES, p.T * p.rows, LANES), F32),
            VMEM((p.Q, p.noct, 2 * half), F32),
            VMEM((p.Q, p.noct, 2 * half), F32),
        ],
        flops=4_000_000_000,
        specs=[smem] + [vmem] * (p.Z + p.Q),
    )(pace, *parts, *sigs)
    bases, (ends, whole, *rest) = results[: p.Q], results[p.Q :]
    wholes = [whole] + [send(whole, p.shift_z(k)) for k in range(1, p.Z)]
    acts = call(
        functools.partial(lift_kernel, p),
        [shape((p.T, p.mine), BF16)] * p.Q,
        [
            VMEM((2 * half // LANES, p.T * p.rows, LANES), F32),
            VMEM((p.Z, p.noct, 2 * half), F32),
            VMEM((3, p.Q, p.noct, 2 * half), F32),
        ],
        flops=3_000_000_000,
    )(ends, *rest, *wholes, *bases)
    acts = [acts[0]] + [send(acts[j], p.swap_q(j)) for j in range(1, p.Q)]
    mixed = call(
        functools.partial(gate_kernel, p, len(glu_units)),
        shape((p.T, p.width), BF16),
        [VMEM((p.Q, p.T, p.mine), BF16), VMEM((p.width, p.width), BF16)],
        flops=2_000_000_000,
    )(b_glu.reshape(1, -1), g_mix.reshape(1, -1), *acts, *glu_units)
    project = call(
        functools.partial(project_kernel, p, len(out_units)),
        shape((p.T, p.X * p.wc), BF16),
        [VMEM((p.X, p.width, p.wc), BF16)],
        flops=2_000_000_000,
    )
    halves = []
    if p.C == 2:
        halves = [send(project(send(mixed, p.swap_q(1)), *out_units), p.swap_q(1))]
    halves = [project(mixed, *out_units)] + halves
    return call(
        functools.partial(merge_kernel, p), shape((1, p.T, p.X * p.C * p.wc), BF16)
    )(*halves)


def solution(mesh):
    in_specs = (
        P("dp", "sp", None),
        P("dp", None),
        P("sp"),
        P("sp", None),
        P("sp", None),
        P("sp", None, None, None),
        P("sp", None, None, None),
        P("sp"),
        P("dp", None, "sp", None),
        P("sp", "dp"),
        P(),
        P(),
        P("sp", "dp"),
    )
    return jax.shard_map(
        functools.partial(layer, mesh),
        mesh=mesh,
        in_specs=in_specs,
        out_specs=P("dp", "sp", None),
        check_vma=False,
    )
```

time: 148 us -> 104 us (0.70)
  blocking collectives: 36.3 us -> 0 us
  other arithmetic: 33.4 us -> 0.3 us
  matrix products: 30.3 us -> 0 us
  Pallas kernels: 0 us -> 25.1 us
  waiting for transfers between devices: 17 us -> 40.8 us
  starting transfers between devices: 6.23 us -> 29.6 us
  between operations: 14.1 us -> 0.35 us
  local copies, waits for them, and re-layouts: 10.5 us -> 7.64 us
    ppermute x0 -> x33, waiting for transfers between devices: none -> 40.8 us  [send(): return lax.ppermute(value, AXES, pairs)]
    dot_general x5 -> x0, matrix products: 30.3 us -> none  [the longest x1 11 us: mix_group(): jnp.einsum('cp,kps->ksc', out_map[1], state_im, precision=highest)]
    ppermute x0 -> x33, starting transfers between devices: none -> 29.6 us  [send(): return lax.ppermute(value, AXES, pairs)]
    pallas_call x0 -> x7, Pallas kernels: none -> 25.1 us  [the longest x1 5.9 us: layer(): call(functools.partial(scan_kernel, p), [shape((p.T, p.mine), F32)] * p.Q...]
    all_to_all x1 -> x0, blocking collectives: 20.1 us -> none  [per_device(): lax.all_to_all(local_act, 'sp', split_axis=1, concat_axis=2, tiled=True)]
    sub x9 -> x0, other arithmetic: 17.9 us -> none  [the longest x7 17.7 us: mix_group(): inner_re + power_re * moved_re - power_im * moved_im]
    all_gather x2 -> x0, blocking collectives: 16.1 us -> none  [the longest x1 8.38 us: per_device(): lax.all_gather(w_out, 'dp', axis=1, tiled=True)]
    unnamed x2 -> x0, other arithmetic: 13.6 us -> none
  transfers between devices with their start and end apart: 3 -> 33, of which waited for: 2 -> 12; matrix products, arithmetic and copies ran while one was open for 46% -> 3% of each run, Pallas kernels for 0% -> 18%
where the time goes in v1:
time: 104 us
  waiting for transfers between devices  40.8 us (39%)
  starting transfers between devices  29.6 us (28%)
  Pallas kernels  25.1 us (24%)
  local copies, waits for them, and re-layouts  7.64 us (7%)
    ppermute x33, waiting for transfers between devices, send(): return lax.ppermute(value, AXES, pairs)  40.8 us
    ppermute x33, starting transfers between devices, send(): return lax.ppermute(value, AXES, pairs)  29.6 us
    unnamed x68, local copies, waits for them, and re-layouts  6.98 us
    pallas_call x1, Pallas kernels, layer(): call(functools.partial(scan_kernel, p), [shape((p.T, p.mine), F32)] * p.Q...  5.9 us
    pallas_call x1, Pallas kernels, layer(): halves = [send(project(send(mixed, p.swap_q(1)), *out_units), p.swap_q(1))]  4.05 us
    pallas_call x1, Pallas kernels, layer(): halves = [project(mixed, *out_units)] + halves  4.03 us
    pallas_call x1, Pallas kernels, layer(): call(functools.partial(lift_kernel, p), [shape((p.T, p.mine), BF16)] * p....  3.51 us
    pallas_call x1, Pallas kernels, layer(): call(functools.partial(gate_kernel, p, len(glu_units)), shape((p.T, p.wid...  3.15 us
  transfers between devices with their start and end apart: 33, of which 12 were waited for; matrix products, arithmetic and copies ran while one was open for 3% of the time, Pallas kernels for 18%

profile of v1, /device:TPU:0, one launch (start us, length us, event | category | flops | bytes accessed | tf_op | source)
XLA Modules:
  0.0 103.8 jit_solution(7066333362407951050)
XLA Ops:
  0.0 5.1 %collective-permute-start.14 = (bf16[64,512]{1,0:T(8,128)(2,1)}, bf16[64,512]{1,0:T(8,128)(2,1)S(1)}, u32[]{:S(2)}, u32[]{:S(2)}) collective-permute-start(bf16[64,512]{1,0:T(8,128)(2,1)} %param.22), channel_id=1, source_target_pairs={{0,24},{1,25},{2,26},{3,27},{4,28},{5,29},{6,30},{7,31},{8,0},{9,1... | collective-permute-start | bytes 196616 | tf_op jit(solution)/shard_map/ppermute | solution.py:109
  5.1 1.0 collective-permute-start.12
  6.1 1.7 %copy.14.in_map = f32[4,2,64,16]{3,2,1,0:T(8,128)} copy(f32[4,2,64,16]{2,3,1,0:T(8,128)} %param.18) | data formatting | bytes 65536 | tf_op args[5]
  9.1 2.2 %shard_map.127 = (bf16[176,128]{1,0:T(8,128)(2,1)}, bf16[64,1024]{1,0:T(8,128)(2,1)}, bf16[64,1024]{1,0:T(8,128)(2,1)}, bf16[128,256]{1,0:T(8,128)(2,1)}, bf16[1...) custom-call(bf16[1,128,1024]{2,1,0:T(8,128)(2,1)} %sig.1, f32[4,2,64,16]{3,2,1,0:T(8,128)} %copy.14.in_map, ...), custom_call_target="tpu_custom_call" | custom-call | flops 1000000 | bytes 1000000 | tf_op jit(solution)/shard_map/pallas_call | solution.py:471
  11.8 1.6 %collective-permute-start.15 = (bf16[4,64,512]{2,1,0:T(8,128)(2,1)S(1)}, bf16[4,64,512]{2,1,0:T(8,128)(2,1)S(1)}, u32[]{:S(2)}, u32[]{:S(2)}) collective-permute-start(bf16[4,64,512]{2,1,0:T(8,128)(2,1)S(1)} %get-tuple-element.50), channel_id=1, source_target_pairs={{0,4},{1,5},{2,3},{3,2},{4,0},{5,1},{6,7},{7,6},{8,12},{9,13},{10,... | collective-permute-start | bytes 786440 | tf_op jit(solution)/shard_map/ppermute | solution.py:109
  13.5 2.1 %collective-permute-start.22 = (bf16[128,1024]{1,0:T(8,128)(2,1)S(1)}, bf16[128,1024]{1,0:T(8,128)(2,1)S(1)}, u32[]{:S(2)}, u32[]{:S(2)}) collective-permute-start(bf16[128,1024]{1,0:T(8,128)(2,1)S(1)} %constant_dynamic-update-slice_fusion), channel_id=1, source_target_pairs={{0,8},{1,9},{2,10},{3,11},{4,12},{5,13},{6,14},{7,15},{8,16},{9,17... | collective-permute-start | bytes 786440 | tf_op jit(solution)/shard_map/ppermute | solution.py:109
  16.3 1.7 %collective-permute-start.1 = (bf16[176,128]{1,0:T(8,128)(2,1)S(1)}, bf16[176,128]{1,0:T(8,128)(2,1)S(1)}, u32[]{:S(2)}, u32[]{:S(2)}) collective-permute-start(bf16[176,128]{1,0:T(8,128)(2,1)S(1)} %copy-done.26), channel_id=1, source_target_pairs={{0,16},{1,17},{2,18},{3,19},{4,20},{5,21},{6,22},{7,23},{8,24},{9,... | collective-permute-start | bytes 135176 | tf_op jit(solution)/shard_map/ppermute | solution.py:109
  17.9 1.5 %collective-permute-start.2 = (bf16[176,128]{1,0:T(8,128)(2,1)S(1)}, bf16[176,128]{1,0:T(8,128)(2,1)S(1)}, u32[]{:S(2)}, u32[]{:S(2)}) collective-permute-start(bf16[176,128]{1,0:T(8,128)(2,1)S(1)} %copy-done.26), channel_id=1, source_target_pairs={{0,24},{1,25},{2,26},{3,27},{4,28},{5,29},{6,30},{7,31},{8,0},{9,1... | collective-permute-start | bytes 135176 | tf_op jit(solution)/shard_map/ppermute | solution.py:109
  19.4 5.9 %collective-permute-done.refs_1_ = bf16[176,128]{1,0:T(8,128)(2,1)S(1)} collective-permute-done((bf16[176,128]{1,0:T(8,128)(2,1)S(1)}, bf16[176,128]{1,0:T(8,128)(2,1)S(1)}, u32[]{:S(2)}, u32[]{:S(2)}) %collective-permute-start) | collective-permute-done | bytes 45088 | tf_op jit(solution)/shard_map/ppermute | solution.py:109
  26.4 1.4 %collective-permute-start.4 = (bf16[128,256]{1,0:T(8,128)(2,1)S(1)}, bf16[128,256]{1,0:T(8,128)(2,1)S(1)}, u32[]{:S(2)}, u32[]{:S(2)}) collective-permute-start(bf16[128,256]{1,0:T(8,128)(2,1)S(1)} %copy-done.15), channel_id=1, source_target_pairs={{0,4},{1,5},{2,6},{3,7},{4,0},{5,1},{6,2},{7,3},{8,12},{9,13},{10,... | collective-permute-start | bytes 196616 | tf_op jit(solution)/shard_map/ppermute | solution.py:109
  27.9 1.5 %collective-permute-start.20 = (bf16[128,1024]{1,0:T(8,128)(2,1)S(1)}, bf16[128,1024]{1,0:T(8,128)(2,1)S(1)}, u32[]{:S(2)}, u32[]{:S(2)}) collective-permute-start(bf16[128,1024]{1,0:T(8,128)(2,1)S(1)} %constant_dynamic-update-slice_fusion), channel_id=1, source_target_pairs={{0,4},{1,5},{2,3},{3,2},{4,0},{5,1},{6,7},{7,6},{8,12},{9,13},{10,... | collective-permute-start | bytes 786440 | tf_op jit(solution)/shard_map/ppermute | solution.py:109
  29.4 1.2 %collective-permute-start.16 = (bf16[2,4,64,512]{3,2,1,0:T(8,128)(2,1)S(1)}, bf16[2,4,64,512]{3,2,1,0:T(8,128)(2,1)S(1)}, u32[]{:S(2)}, u32[]{:S(2)}) collective-permute-start(bf16[2,4,64,512]{3,2,1,0:T(8,128)(2,1)S(1)} %pad_maximum_fusion.refs_4_), channel_id=1, source_target_pairs={{0,1},{1,0},{2,6},{3,7},{4,5},{5,4},{6,2},{7,3},{8,9},{9,8},{10,14... | collective-permute-start | bytes 1572872 | tf_op jit(solution)/shard_map/ppermute | solution.py:109
  30.7 1.5 %collective-permute-done.5.refs_7_ = bf16[128,256]{1,0:T(8,128)(2,1)S(1)} collective-permute-done((bf16[128,256]{1,0:T(8,128)(2,1)S(1)}, bf16[128,256]{1,0:T(8,128)(2,1)S(1)}, u32[]{:S(2)}, u32[]{:S(2)}) %collective-permute-start.5) | collective-permute-done | bytes 65568 | tf_op jit(solution)/shard_map/ppermute | solution.py:109
  32.8 5.9 %shard_map.128 = (f32[128,256]{1,0:T(8,128)}, f32[128,256]{1,0:T(8,128)}, f32[128,256]{1,0:T(8,128)}, f32[128,256]{1,0:T(8,128)}, f32[8,1024]{1,0:T(8,128)}, /*i...) custom-call(f32[1,16]{1,0:T(1,128)} %pace.1, ...), custom_call_target="tpu_custom_call" | custom-call | flops 4000000000 | bytes 1000000 | tf_op jit(solution)/shard_map/pallas_call | solution.py:504
  38.9 2.7 %collective-permute-start.7 = (f32[2,1024]{1,0:T(2,128)}, f32[2,1024]{1,0:T(2,128)S(1)}, u32[]{:S(2)}, u32[]{:S(2)}) collective-permute-start(f32[2,1024]{1,0:T(2,128)} %get-tuple-element.38.refs_0_), channel_id=1, source_target_pairs={{0,16},{1,17},{2,18},{3,19},{4,20},{5,21},{6,22},{7,23},{8,24},{9,... | collective-permute-start | bytes 24584 | tf_op jit(solution)/shard_map/ppermute | solution.py:109
  41.6 2.8 %collective-permute-done.6.refs_1_ = f32[2,1024]{1,0:T(2,128)S(1)} collective-permute-done((f32[2,1024]{1,0:T(2,128)}, f32[2,1024]{1,0:T(2,128)S(1)}, u32[]{:S(2)}, u32[]{:S(2)}) %collective-permute-start.6) | collective-permute-done | bytes 8224 | tf_op jit(solution)/shard_map/ppermute | solution.py:109
  45.0 3.3 %collective-permute-done.8.refs_3_ = f32[2,1024]{1,0:T(2,128)S(1)} collective-permute-done((f32[2,1024]{1,0:T(2,128)}, f32[2,1024]{1,0:T(2,128)S(1)}, u32[]{:S(2)}, u32[]{:S(2)}) %collective-permute-start.8) | collective-permute-done | bytes 8224 | tf_op jit(solution)/shard_map/ppermute | solution.py:109
  48.9 1.4 %collective-permute-start.26 = (bf16[128,1024]{1,0:T(8,128)(2,1)S(1)}, bf16[128,1024]{1,0:T(8,128)(2,1)S(1)}, u32[]{:S(2)}, u32[]{:S(2)}) collective-permute-start(bf16[128,1024]{1,0:T(8,128)(2,1)S(1)} %collective-permute-done.25), channel_id=1, source_target_pairs={{0,4},{1,5},{2,3},{3,2},{4,0},{5,1},{6,7},{7,6},{8,12},{9,13},{10,... | collective-permute-start | bytes 786440 | tf_op jit(solution)/shard_map/ppermute | solution.py:109
  50.4 3.5 %shard_map.129 = (bf16[128,256]{1,0:T(8,128)(2,1)}, bf16[128,256]{1,0:T(8,128)(2,1)}, bf16[128,256]{1,0:T(8,128)(2,1)}, bf16[128,256]{1,0:T(8,128)(2,1)}) custom-call(f32[8,1024]{1,0:T(8,128)} %get-tuple-element.32.ends, f32[8,1024]{1,0:T(8,128)} %get-tuple-element.33.bars, f32[8,1024]{1,0:T(8,128)} %get-tuple-element.34.blocks, ...), custom_call_target="tpu_custom_call" | custom-call | flops 3000000000 | bytes 1000000 | tf_op jit(solution)/shard_map/pallas_call | solution.py:528
  54.0 4.5 %collective-permute-done.28 = bf16[128,1024]{1,0:T(8,128)(2,1)S(1)} collective-permute-done((bf16[128,1024]{1,0:T(8,128)(2,1)S(1)}, bf16[128,1024]{1,0:T(8,128)(2,1)S(1)}, u32[]{:S(2)}, u32[]{:S(2)}) %collective-permute-start.28) | collective-permute-done | bytes 262176 | tf_op jit(solution)/shard_map/ppermute | solution.py:109
  60.8 1.4 %collective-permute-start.10 = (bf16[128,256]{1,0:T(8,128)(2,1)S(1)}, bf16[128,256]{1,0:T(8,128)(2,1)S(1)}, u32[]{:S(2)}, u32[]{:S(2)}) collective-permute-start(bf16[128,256]{1,0:T(8,128)(2,1)S(1)} %copy-done.18), channel_id=1, source_target_pairs={{0,4},{1,5},{2,6},{3,7},{4,0},{5,1},{6,2},{7,3},{8,12},{9,13},{10,... | collective-permute-start | bytes 196616 | tf_op jit(solution)/shard_map/ppermute | solution.py:109
  62.3 3.3 %collective-permute-done.29 = bf16[128,1024]{1,0:T(8,128)(2,1)S(1)} collective-permute-done((bf16[128,1024]{1,0:T(8,128)(2,1)S(1)}, bf16[128,1024]{1,0:T(8,128)(2,1)S(1)}, u32[]{:S(2)}, u32[]{:S(2)}) %collective-permute-start.29) | collective-permute-done | bytes 262176 | tf_op jit(solution)/shard_map/ppermute | solution.py:109
  65.7 1.4 %collective-permute-start.21 = (bf16[2,128,1024]{2,1,0:T(8,128)(2,1)S(1)}, bf16[2,128,1024]{2,1,0:T(8,128)(2,1)S(1)}, u32[]{:S(2)}, u32[]{:S(2)}) collective-permute-start(bf16[2,128,1024]{2,1,0:T(8,128)(2,1)S(1)} %pad_maximum_fusion.1.refs_0_), channel_id=1, source_target_pairs={{0,1},{1,0},{2,6},{3,7},{4,5},{5,4},{6,2},{7,3},{8,9},{9,8},{10,14... | collective-permute-start | bytes 1572872 | tf_op jit(solution)/shard_map/ppermute | solution.py:109
  67.8 1.4 %collective-permute-done.11.refs_3_ = bf16[128,256]{1,0:T(8,128)(2,1)S(1)} collective-permute-done((bf16[128,256]{1,0:T(8,128)(2,1)S(1)}, bf16[128,256]{1,0:T(8,128)(2,1)S(1)}, u32[]{:S(2)}, u32[]{:S(2)}) %collective-permute-start.11) | collective-permute-done | bytes 65568 | tf_op jit(solution)/shard_map/ppermute | solution.py:109
  69.3 1.4 %collective-permute-start.27 = (bf16[2,128,1024]{2,1,0:T(8,128)(2,1)S(1)}, bf16[2,128,1024]{2,1,0:T(8,128)(2,1)}, u32[]{:S(2)}, u32[]{:S(2)}) collective-permute-start(bf16[2,128,1024]{2,1,0:T(8,128)(2,1)S(1)} %pad_maximum_fusion.3.refs_4_), channel_id=1, source_target_pairs={{0,1},{1,0},{2,6},{3,7},{4,5},{5,4},{6,2},{7,3},{8,9},{9,8},{10,14... | collective-permute-start | bytes 1572872 | tf_op jit(solution)/shard_map/ppermute | solution.py:109
  72.1 3.2 %shard_map.130.mixed = bf16[128,1024]{1,0:T(8,128)(2,1)} custom-call(f32[1,1024]{1,0:T(1,128)} %bitcast.34, f32[1,1024]{1,0:T(1,128)} %bitcast.35, bf16[128,256]{1,0:T(8,128)(2,1)} %get-tuple-element.43.refs_0_, bf16[128,256]{1,0:T(8,128)(2,1)} %copy-done.21, bf16[128,256]{1,0:T(8,128)(2,1)} %copy-done.23, bf16[128,256]{1,0:T(8,128)(2,1)} %copy-done.25, ...), custom_call_target="tpu_custom_call" | custom-call | flops 2000000000 | bytes 1000000 | tf_op jit(solution)/shard_map/pallas_call | solution.py:539
  75.3 5.3 %collective-permute-done.24.refs_3_ = bf16[2,128,1024]{2,1,0:T(8,128)(2,1)} collective-permute-done((bf16[2,128,1024]{2,1,0:T(8,128)(2,1)S(1)}, bf16[2,128,1024]{2,1,0:T(8,128)(2,1)}, u32[]{:S(2)}, u32[]{:S(2)}) %collective-permute-start.24) | collective-permute-done | bytes 524320 | tf_op jit(solution)/shard_map/ppermute | solution.py:109
  80.6 5.6 %collective-permute-done.27.refs_5_ = bf16[2,128,1024]{2,1,0:T(8,128)(2,1)} collective-permute-done((bf16[2,128,1024]{2,1,0:T(8,128)(2,1)S(1)}, bf16[2,128,1024]{2,1,0:T(8,128)(2,1)}, u32[]{:S(2)}, u32[]{:S(2)}) %collective-permute-start.27) | collective-permute-done | bytes 524320 | tf_op jit(solution)/shard_map/ppermute | solution.py:109
  86.3 5.5 %collective-permute-done.30.refs_7_ = bf16[2,128,1024]{2,1,0:T(8,128)(2,1)S(1)} collective-permute-done((bf16[2,128,1024]{2,1,0:T(8,128)(2,1)S(1)}, bf16[2,128,1024]{2,1,0:T(8,128)(2,1)S(1)}, u32[]{:S(2)}, u32[]{:S(2)}) %collective-permute-start.30) | collective-permute-done | bytes 524320 | tf_op jit(solution)/shard_map/ppermute | solution.py:109
  92.6 4.1 %shard_map.132 = bf16[128,2048]{1,0:T(8,128)(2,1)} custom-call(bf16[128,1024]{1,0:T(8,128)(2,1)} %copy-done.13, bf16[2,128,1024]{2,1,0:T(8,128)(2,1)} %copy-done.1, bf16[2,128,1024]{2,1,0:T(8,128)(2,1)} %copy-done.11, bf16[2,128,1024]{2,1,0:T(8,128)(2,1)} %copy-done.2, bf16[2,128,1024]{2,1,0:T(8,128)(2,1)} %collective-permute-done.24.refs_3_, ...), custom_call_target="tpu_custom_call" | custom-call | flops 2000000000 | bytes 1000000 | tf_op jit(solution)/shard_map/pallas_call | solution.py:553
  96.7 4.0 %shard_map.131.refs_0_ = bf16[128,2048]{1,0:T(8,128)(2,1)} custom-call(bf16[128,1024]{1,0:T(8,128)(2,1)} %shard_map.130.mixed, bf16[2,128,1024]{2,1,0:T(8,128)(2,1)} %copy-done.1, bf16[2,128,1024]{2,1,0:T(8,128)(2,1)} %copy-done.11, bf16[2,128,1024]{2,1,0:T(8,128)(2,1)} %copy-done.2, bf16[2,128,1024]{2,1,0:T(8,128)(2,1)} %collective-permute-done.24.refs_3_, ...), custom_call_target="tpu_custom_call" | custom-call | flops 2000000000 | bytes 1000000 | tf_op jit(solution)/shard_map/pallas_call | solution.py:554
  101.6 2.3 %shard_map.133 = bf16[1,128,4096]{2,1,0:T(8,128)(2,1)} custom-call(bf16[128,2048]{1,0:T(8,128)(2,1)} %shard_map.131.refs_0_, bf16[128,2048]{1,0:T(8,128)(2,1)} %copy-done.5), custom_call_target="tpu_custom_call" | custom-call | flops 1000000 | bytes 1000000 | tf_op jit(solution)/shard_map/pallas_call | solution.py:555
  (117 shorter events, 11.9 us)
Async XLA Ops:
  0.0 11.3 %collective-permute-start.14 = (bf16[64,512]{1,0:T(8,128)(2,1)}, bf16[64,512]{1,0:T(8,128)(2,1)S(1)}, u32[]{:S(2)}, u32[]{:S(2)}) collective-permute-start(bf16[64,512]{1,0:T(8,128)(2,1)} %param.22), channel_id=1, source_target_pairs={{0,24},{1,25},{2,26},{3,27},{4,28},{5,29},{6,30},{7,31},{8,0},{9,1... | collective-permute-start | bytes 196616 | tf_op jit(solution)/shard_map/ppermute | solution.py:109
  5.1 6.7 %collective-permute-start.13 = (bf16[64,512]{1,0:T(8,128)(2,1)}, bf16[64,512]{1,0:T(8,128)(2,1)S(1)}, u32[]{:S(2)}, u32[]{:S(2)}) collective-permute-start(bf16[64,512]{1,0:T(8,128)(2,1)} %param.22), channel_id=1, source_target_pairs={{0,16},{1,17},{2,18},{3,19},{4,20},{5,21},{6,22},{7,23},{8,24},{9,... | collective-permute-start | bytes 196616 | tf_op jit(solution)/shard_map/ppermute | solution.py:109
  5.1 6.7 %collective-permute-start.12 = (bf16[64,512]{1,0:T(8,128)(2,1)}, bf16[64,512]{1,0:T(8,128)(2,1)S(1)}, u32[]{:S(2)}, u32[]{:S(2)}) collective-permute-start(bf16[64,512]{1,0:T(8,128)(2,1)} %param.22), channel_id=1, source_target_pairs={{0,8},{1,9},{2,10},{3,11},{4,12},{5,13},{6,14},{7,15},{8,16},{9,17... | collective-permute-start | bytes 196616 | tf_op jit(solution)/shard_map/ppermute | solution.py:109
  11.8 16.0 %collective-permute-start.15 = (bf16[4,64,512]{2,1,0:T(8,128)(2,1)S(1)}, bf16[4,64,512]{2,1,0:T(8,128)(2,1)S(1)}, u32[]{:S(2)}, u32[]{:S(2)}) collective-permute-start(bf16[4,64,512]{2,1,0:T(8,128)(2,1)S(1)} %get-tuple-element.50), channel_id=1, source_target_pairs={{0,4},{1,5},{2,3},{3,2},{4,0},{5,1},{6,7},{7,6},{8,12},{9,13},{10,... | collective-permute-start | bytes 786440 | tf_op jit(solution)/shard_map/ppermute | solution.py:109
  13.5 17.1 %collective-permute-start.22 = (bf16[128,1024]{1,0:T(8,128)(2,1)S(1)}, bf16[128,1024]{1,0:T(8,128)(2,1)S(1)}, u32[]{:S(2)}, u32[]{:S(2)}) collective-permute-start(bf16[128,1024]{1,0:T(8,128)(2,1)S(1)} %constant_dynamic-update-slice_fusion), channel_id=1, source_target_pairs={{0,8},{1,9},{2,10},{3,11},{4,12},{5,13},{6,14},{7,15},{8,16},{9,17... | collective-permute-start | bytes 786440 | tf_op jit(solution)/shard_map/ppermute | solution.py:109
  15.6 9.7 %collective-permute-start = (bf16[176,128]{1,0:T(8,128)(2,1)S(1)}, bf16[176,128]{1,0:T(8,128)(2,1)S(1)}, u32[]{:S(2)}, u32[]{:S(2)}) collective-permute-start(bf16[176,128]{1,0:T(8,128)(2,1)S(1)} %copy-done.26), channel_id=1, source_target_pairs={{0,8},{1,9},{2,10},{3,11},{4,12},{5,13},{6,14},{7,15},{8,16},{9,17... | collective-permute-start | bytes 135176 | tf_op jit(solution)/shard_map/ppermute | solution.py:109
  16.3 10.1 %collective-permute-start.1 = (bf16[176,128]{1,0:T(8,128)(2,1)S(1)}, bf16[176,128]{1,0:T(8,128)(2,1)S(1)}, u32[]{:S(2)}, u32[]{:S(2)}) collective-permute-start(bf16[176,128]{1,0:T(8,128)(2,1)S(1)} %copy-done.26), channel_id=1, source_target_pairs={{0,16},{1,17},{2,18},{3,19},{4,20},{5,21},{6,22},{7,23},{8,24},{9,... | collective-permute-start | bytes 135176 | tf_op jit(solution)/shard_map/ppermute | solution.py:109
  17.9 10.0 %collective-permute-start.2 = (bf16[176,128]{1,0:T(8,128)(2,1)S(1)}, bf16[176,128]{1,0:T(8,128)(2,1)S(1)}, u32[]{:S(2)}, u32[]{:S(2)}) collective-permute-start(bf16[176,128]{1,0:T(8,128)(2,1)S(1)} %copy-done.26), channel_id=1, source_target_pairs={{0,24},{1,25},{2,26},{3,27},{4,28},{5,29},{6,30},{7,31},{8,0},{9,1... | collective-permute-start | bytes 135176 | tf_op jit(solution)/shard_map/ppermute | solution.py:109
  25.3 4.1 %collective-permute-start.3 = (bf16[128,256]{1,0:T(8,128)(2,1)S(1)}, bf16[128,256]{1,0:T(8,128)(2,1)S(1)}, u32[]{:S(2)}, u32[]{:S(2)}) collective-permute-start(bf16[128,256]{1,0:T(8,128)(2,1)S(1)} %copy-done.16), channel_id=1, source_target_pairs={{0,2},{1,3},{2,0},{3,1},{4,6},{5,7},{6,4},{7,5},{8,10},{9,11},{10,... | collective-permute-start | bytes 196616 | tf_op jit(solution)/shard_map/ppermute | solution.py:109
  26.4 4.3 %collective-permute-start.4 = (bf16[128,256]{1,0:T(8,128)(2,1)S(1)}, bf16[128,256]{1,0:T(8,128)(2,1)S(1)}, u32[]{:S(2)}, u32[]{:S(2)}) collective-permute-start(bf16[128,256]{1,0:T(8,128)(2,1)S(1)} %copy-done.15), channel_id=1, source_target_pairs={{0,4},{1,5},{2,6},{3,7},{4,0},{5,1},{6,2},{7,3},{8,12},{9,13},{10,... | collective-permute-start | bytes 196616 | tf_op jit(solution)/shard_map/ppermute | solution.py:109
  27.8 4.4 %collective-permute-start.5 = (bf16[128,256]{1,0:T(8,128)(2,1)S(1)}, bf16[128,256]{1,0:T(8,128)(2,1)S(1)}, u32[]{:S(2)}, u32[]{:S(2)}) collective-permute-start(bf16[128,256]{1,0:T(8,128)(2,1)S(1)} %copy-done.14), channel_id=1, source_target_pairs={{0,6},{1,7},{2,4},{3,5},{4,2},{5,3},{6,0},{7,1},{8,14},{9,15},{10,... | collective-permute-start | bytes 196616 | tf_op jit(solution)/shard_map/ppermute | solution.py:109
  27.9 22.4 %collective-permute-start.20 = (bf16[128,1024]{1,0:T(8,128)(2,1)S(1)}, bf16[128,1024]{1,0:T(8,128)(2,1)S(1)}, u32[]{:S(2)}, u32[]{:S(2)}) collective-permute-start(bf16[128,1024]{1,0:T(8,128)(2,1)S(1)} %constant_dynamic-update-slice_fusion), channel_id=1, source_target_pairs={{0,4},{1,5},{2,3},{3,2},{4,0},{5,1},{6,7},{7,6},{8,12},{9,13},{10,... | collective-permute-start | bytes 786440 | tf_op jit(solution)/shard_map/ppermute | solution.py:109
  29.4 24.5 %collective-permute-start.16 = (bf16[2,4,64,512]{3,2,1,0:T(8,128)(2,1)S(1)}, bf16[2,4,64,512]{3,2,1,0:T(8,128)(2,1)S(1)}, u32[]{:S(2)}, u32[]{:S(2)}) collective-permute-start(bf16[2,4,64,512]{3,2,1,0:T(8,128)(2,1)S(1)} %pad_maximum_fusion.refs_4_), channel_id=1, source_target_pairs={{0,1},{1,0},{2,6},{3,7},{4,5},{5,4},{6,2},{7,3},{8,9},{9,8},{10,14... | collective-permute-start | bytes 1572872 | tf_op jit(solution)/shard_map/ppermute | solution.py:109
  30.6 18.3 %collective-permute-start.25 = (bf16[128,1024]{1,0:T(8,128)(2,1)S(1)}, bf16[128,1024]{1,0:T(8,128)(2,1)S(1)}, u32[]{:S(2)}, u32[]{:S(2)}) collective-permute-start(bf16[128,1024]{1,0:T(8,128)(2,1)S(1)} %collective-permute-done.22), channel_id=1, source_target_pairs={{0,8},{1,9},{2,10},{3,11},{4,12},{5,13},{6,14},{7,15},{8,16},{9,17... | collective-permute-start | bytes 786440 | tf_op jit(solution)/shard_map/ppermute | solution.py:109
  38.7 5.7 %collective-permute-start.6 = (f32[2,1024]{1,0:T(2,128)}, f32[2,1024]{1,0:T(2,128)S(1)}, u32[]{:S(2)}, u32[]{:S(2)}) collective-permute-start(f32[2,1024]{1,0:T(2,128)} %get-tuple-element.38.refs_0_), channel_id=1, source_target_pairs={{0,8},{1,9},{2,10},{3,11},{4,12},{5,13},{6,14},{7,15},{8,16},{9,17... | collective-permute-start | bytes 24584 | tf_op jit(solution)/shard_map/ppermute | solution.py:109
  38.9 6.0 %collective-permute-start.7 = (f32[2,1024]{1,0:T(2,128)}, f32[2,1024]{1,0:T(2,128)S(1)}, u32[]{:S(2)}, u32[]{:S(2)}) collective-permute-start(f32[2,1024]{1,0:T(2,128)} %get-tuple-element.38.refs_0_), channel_id=1, source_target_pairs={{0,16},{1,17},{2,18},{3,19},{4,20},{5,21},{6,22},{7,23},{8,24},{9,... | collective-permute-start | bytes 24584 | tf_op jit(solution)/shard_map/ppermute | solution.py:109
  44.4 3.9 %collective-permute-start.8 = (f32[2,1024]{1,0:T(2,128)}, f32[2,1024]{1,0:T(2,128)S(1)}, u32[]{:S(2)}, u32[]{:S(2)}) collective-permute-start(f32[2,1024]{1,0:T(2,128)} %get-tuple-element.38.refs_0_), channel_id=1, source_target_pairs={{0,24},{1,25},{2,26},{3,27},{4,28},{5,29},{6,30},{7,31},{8,0},{9,1... | collective-permute-start | bytes 24584 | tf_op jit(solution)/shard_map/ppermute | solution.py:109
  44.9 25.7 %collective-permute-start.17 = (bf16[2,4,64,512]{3,2,1,0:T(8,128)(2,1)S(1)}, bf16[2,4,64,512]{3,2,1,0:T(8,128)(2,1)}, u32[]{:S(2)}, u32[]{:S(2)}) collective-permute-start(bf16[2,4,64,512]{3,2,1,0:T(8,128)(2,1)S(1)} %pad_maximum_fusion.refs_4_), channel_id=1, source_target_pairs={{0,2},{1,3},{2,0},{3,1},{4,6},{5,7},{6,4},{7,5},{8,10},{9,11},{10,... | collective-permute-start | bytes 1572872 | tf_op jit(solution)/shard_map/ppermute | solution.py:109
  48.3 10.9 %collective-permute-start.23 = (bf16[128,1024]{1,0:T(8,128)(2,1)S(1)}, bf16[128,1024]{1,0:T(8,128)(2,1)S(1)}, u32[]{:S(2)}, u32[]{:S(2)}) collective-permute-start(bf16[128,1024]{1,0:T(8,128)(2,1)S(1)} %collective-permute-done.22), channel_id=1, source_target_pairs={{0,4},{1,5},{2,3},{3,2},{4,0},{5,1},{6,7},{7,6},{8,12},{9,13},{10,... | collective-permute-start | bytes 786440 | tf_op jit(solution)/shard_map/ppermute | solution.py:109
  48.9 11.1 %collective-permute-start.26 = (bf16[128,1024]{1,0:T(8,128)(2,1)S(1)}, bf16[128,1024]{1,0:T(8,128)(2,1)S(1)}, u32[]{:S(2)}, u32[]{:S(2)}) collective-permute-start(bf16[128,1024]{1,0:T(8,128)(2,1)S(1)} %collective-permute-done.25), channel_id=1, source_target_pairs={{0,4},{1,5},{2,3},{3,2},{4,0},{5,1},{6,7},{7,6},{8,12},{9,13},{10,... | collective-permute-start | bytes 786440 | tf_op jit(solution)/shard_map/ppermute | solution.py:109
  50.3 8.2 %collective-permute-start.28 = (bf16[128,1024]{1,0:T(8,128)(2,1)S(1)}, bf16[128,1024]{1,0:T(8,128)(2,1)S(1)}, u32[]{:S(2)}, u32[]{:S(2)}) collective-permute-start(bf16[128,1024]{1,0:T(8,128)(2,1)S(1)} %collective-permute-done.25), channel_id=1, source_target_pairs={{0,8},{1,9},{2,10},{3,11},{4,12},{5,13},{6,14},{7,15},{8,16},{9,17... | collective-permute-start | bytes 786440 | tf_op jit(solution)/shard_map/ppermute | solution.py:109
  53.9 17.4 %collective-permute-start.18 = (bf16[2,4,64,512]{3,2,1,0:T(8,128)(2,1)S(1)}, bf16[2,4,64,512]{3,2,1,0:T(8,128)(2,1)S(1)}, u32[]{:S(2)}, u32[]{:S(2)}) collective-permute-start(bf16[2,4,64,512]{3,2,1,0:T(8,128)(2,1)S(1)} %collective-permute-done.16.refs_5_), channel_id=1, source_target_pairs={{0,2},{1,3},{2,0},{3,1},{4,6},{5,7},{6,4},{7,5},{8,10},{9,11},{10,... | collective-permute-start | bytes 1572872 | tf_op jit(solution)/shard_map/ppermute | solution.py:109
  58.5 7.1 %collective-permute-start.29 = (bf16[128,1024]{1,0:T(8,128)(2,1)S(1)}, bf16[128,1024]{1,0:T(8,128)(2,1)S(1)}, u32[]{:S(2)}, u32[]{:S(2)}) collective-permute-start(bf16[128,1024]{1,0:T(8,128)(2,1)S(1)} %collective-permute-done.28), channel_id=1, source_target_pairs={{0,4},{1,5},{2,3},{3,2},{4,0},{5,1},{6,7},{7,6},{8,12},{9,13},{10,... | collective-permute-start | bytes 786440 | tf_op jit(solution)/shard_map/ppermute | solution.py:109
  59.9 5.7 %collective-permute-start.9 = (bf16[128,256]{1,0:T(8,128)(2,1)S(1)}, bf16[128,256]{1,0:T(8,128)(2,1)S(1)}, u32[]{:S(2)}, u32[]{:S(2)}) collective-permute-start(bf16[128,256]{1,0:T(8,128)(2,1)S(1)} %copy-done.20), channel_id=1, source_target_pairs={{0,2},{1,3},{2,0},{3,1},{4,6},{5,7},{6,4},{7,5},{8,10},{9,11},{10,... | collective-permute-start | bytes 196616 | tf_op jit(solution)/shard_map/ppermute | solution.py:109
  60.8 6.3 %collective-permute-start.10 = (bf16[128,256]{1,0:T(8,128)(2,1)S(1)}, bf16[128,256]{1,0:T(8,128)(2,1)S(1)}, u32[]{:S(2)}, u32[]{:S(2)}) collective-permute-start(bf16[128,256]{1,0:T(8,128)(2,1)S(1)} %copy-done.18), channel_id=1, source_target_pairs={{0,4},{1,5},{2,6},{3,7},{4,0},{5,1},{6,2},{7,3},{8,12},{9,13},{10,... | collective-permute-start | bytes 196616 | tf_op jit(solution)/shard_map/ppermute | solution.py:109
  65.6 3.7 %collective-permute-start.11 = (bf16[128,256]{1,0:T(8,128)(2,1)S(1)}, bf16[128,256]{1,0:T(8,128)(2,1)S(1)}, u32[]{:S(2)}, u32[]{:S(2)}) collective-permute-start(bf16[128,256]{1,0:T(8,128)(2,1)S(1)} %copy-done.17), channel_id=1, source_target_pairs={{0,6},{1,7},{2,4},{3,5},{4,2},{5,3},{6,0},{7,1},{8,14},{9,15},{10,... | collective-permute-start | bytes 196616 | tf_op jit(solution)/shard_map/ppermute | solution.py:109
  65.7 9.6 %collective-permute-start.21 = (bf16[2,128,1024]{2,1,0:T(8,128)(2,1)S(1)}, bf16[2,128,1024]{2,1,0:T(8,128)(2,1)S(1)}, u32[]{:S(2)}, u32[]{:S(2)}) collective-permute-start(bf16[2,128,1024]{2,1,0:T(8,128)(2,1)S(1)} %pad_maximum_fusion.1.refs_0_), channel_id=1, source_target_pairs={{0,1},{1,0},{2,6},{3,7},{4,5},{5,4},{6,2},{7,3},{8,9},{9,8},{10,14... | collective-permute-start | bytes 1572872 | tf_op jit(solution)/shard_map/ppermute | solution.py:109
  67.1 13.5 %collective-permute-start.24 = (bf16[2,128,1024]{2,1,0:T(8,128)(2,1)S(1)}, bf16[2,128,1024]{2,1,0:T(8,128)(2,1)}, u32[]{:S(2)}, u32[]{:S(2)}) collective-permute-start(bf16[2,128,1024]{2,1,0:T(8,128)(2,1)S(1)} %pad_maximum_fusion.2.refs_2_), channel_id=1, source_target_pairs={{0,1},{1,0},{2,6},{3,7},{4,5},{5,4},{6,2},{7,3},{8,9},{9,8},{10,14... | collective-permute-start | bytes 1572872 | tf_op jit(solution)/shard_map/ppermute | solution.py:109
  69.3 17.0 %collective-permute-start.27 = (bf16[2,128,1024]{2,1,0:T(8,128)(2,1)S(1)}, bf16[2,128,1024]{2,1,0:T(8,128)(2,1)}, u32[]{:S(2)}, u32[]{:S(2)}) collective-permute-start(bf16[2,128,1024]{2,1,0:T(8,128)(2,1)S(1)} %pad_maximum_fusion.3.refs_4_), channel_id=1, source_target_pairs={{0,1},{1,0},{2,6},{3,7},{4,5},{5,4},{6,2},{7,3},{8,9},{9,8},{10,14... | collective-permute-start | bytes 1572872 | tf_op jit(solution)/shard_map/ppermute | solution.py:109
  70.6 21.1 %collective-permute-start.30 = (bf16[2,128,1024]{2,1,0:T(8,128)(2,1)S(1)}, bf16[2,128,1024]{2,1,0:T(8,128)(2,1)S(1)}, u32[]{:S(2)}, u32[]{:S(2)}) collective-permute-start(bf16[2,128,1024]{2,1,0:T(8,128)(2,1)S(1)} %pad_maximum_fusion.4.refs_6_), channel_id=1, source_target_pairs={{0,1},{1,0},{2,6},{3,7},{4,5},{5,4},{6,2},{7,3},{8,9},{9,8},{10,14... | collective-permute-start | bytes 1572872 | tf_op jit(solution)/shard_map/ppermute | solution.py:109
  75.3 11.0 %collective-permute-start.31 = (bf16[128,1024]{1,0:T(8,128)(2,1)}, bf16[128,1024]{1,0:T(8,128)(2,1)S(1)}, u32[]{:S(2)}, u32[]{:S(2)}) collective-permute-start(bf16[128,1024]{1,0:T(8,128)(2,1)} %shard_map.130.mixed), channel_id=1, source_target_pairs={{0,2},{1,3},{2,0},{3,1},{4,6},{5,7},{6,4},{7,5},{8,10},{9,11},{10,... | collective-permute-start | bytes 786440 | tf_op jit(solution)/shard_map/ppermute | solution.py:109
  96.6 4.1 %collective-permute-start.32 = (bf16[128,2048]{1,0:T(8,128)(2,1)}, bf16[128,2048]{1,0:T(8,128)(2,1)S(1)}, u32[]{:S(2)}, u32[]{:S(2)}) collective-permute-start(bf16[128,2048]{1,0:T(8,128)(2,1)} %shard_map.132), channel_id=1, source_target_pairs={{0,2},{1,3},{2,0},{3,1},{4,6},{5,7},{6,4},{7,5},{8,10},{9,11},{10,... | collective-permute-start | bytes 1572872 | tf_op jit(solution)/shard_map/ppermute | solution.py:109
  (34 other events, 171.6 us)
